TPU v7x, 32 devices: a whole 2x2x4 slice. The times are simulated.
32 devices in a mesh: dp: 2 (over x), kv: 8 (over z, y), tp: 2 (over core).
Axes of the slice: x: 2, y: 2, z: 4, core: 2. Of those that a mesh axis runs over, the one named last changes fastest.
Arguments:
- tokens: bfloat16 [32, 16, 2048], P('dp', None, ('kv', 'tp')), may hold values from -190 to 190
- gain_in: float32 [2048], P(('kv', 'tp')), may hold values from 0.1 to 1.9
- w_qdown: bfloat16 [2048, 512], P(('kv', 'tp')), may hold values from -0.125 to 0.125
- w_kvdown: bfloat16 [2048, 256], P(('kv', 'tp')), may hold values from -0.125 to 0.125
- w_ropek: bfloat16 [2048, 32], replicated, may hold values from -0.125 to 0.125
- gain_qlat: float32 [512], replicated, may hold values from 0.1 to 1.9
- gain_kvlat: float32 [256], replicated, may hold values from 0.1 to 1.9
- w_qup: bfloat16 [512, 16, 96], P(None, 'tp'), may hold values from -0.25 to 0.25
- gain_q: float32 [96], replicated, may hold values from 0.4 to 20
- w_ukey: bfloat16 [256, 16, 64], P(None, 'tp'), may hold values from -0.75 to 0.75
- w_uval: bfloat16 [256, 16, 128], P(None, 'tp'), may hold values from -0.375 to 0.375
- w_out: bfloat16 [2048, 2048], P('tp', 'kv'), may hold values from -2.5 to 2.5
- gain_out: float32 [2048], P(('kv', 'tp')), may hold values from 0.1 to 1.9
- cache_lat: bfloat16 [32, 2048, 256], P('dp', 'kv'), may hold values from -6 to 6
- cache_rope: bfloat16 [32, 32, 2048], P('dp', None, 'kv'), may hold values from -6 to 6
- parents: int32 [32, 16], P('dp'), may hold values from -1 to 14, as said below
- lengths: int32 [32], P('dp'), may hold values from 1024 to 2016
- accepted: int32 [32], P('dp'), may hold values from 0 to 16
Outputs:
- attn_out: bfloat16 [32, 16, 2048], P('dp', None, ('kv', 'tp'))
- lat_cache_out: bfloat16 [32, 2048, 256], P('dp', 'kv')
- rope_cache_out: bfloat16 [32, 32, 2048], P('dp', None, 'kv')
Inputs may be any that keep to these rules, and one draw needn't show every extreme that they name: `parents`: proposal j's parent is -1 (the last accepted token) or a proposal before j. Rows 0 .. lengths + accepted - 1 of a sequence's cache hold its past; the 16 positions after them lie inside the cache.
All inputs are finite; a program needn't handle non-finite values.
Results may differ from a plain program's by a relative error of at most 0.0102.
The roundings to bfloat16 on the way count: a program that leaves them out, or rounds other values in their place, can miss the bound.
Values may be sent and summed in bfloat16 or wider, within the bound.
A program may use at most 64 MiB of HBM per device.

v0:
```python
import jax
import jax.numpy as jnp
from jax import lax
from jax.sharding import PartitionSpec as P

epsilon = 1e-06


def normed(values, gain_vec):
    return (
        values * lax.rsqrt(jnp.mean(values * values, axis=-1, keepdims=True) + epsilon) * gain_vec
    )


def rope_angles(position, half_dim):
    frequency = 10000.0 ** (-(jnp.arange(half_dim, dtype=jnp.float32) * 2.0) / (2 * half_dim))
    return position.astype(jnp.float32)[..., None] * frequency


def ancestry(parents):
    proposals = parents.shape[-1]
    parent_link = (parents[..., :, None] == jnp.arange(proposals, dtype=jnp.int32)).astype(
        jnp.float32
    )
    identity = jnp.broadcast_to(jnp.eye(proposals, dtype=jnp.float32), parent_link.shape)

    def extend(iteration, state_pair):
        reaches, current = state_pair
        current = jnp.einsum("sij,sjk->sik", current, parent_link, precision=lax.Precision.HIGHEST)
        return (reaches + current, current)

    reaches, current = lax.fori_loop(0, proposals - 1, extend, (identity, identity))
    depths = (jnp.sum(reaches, axis=-1) - 1.0).astype(jnp.int32)
    return (reaches, depths)


def latents(summed, squares, full_width, gain_qlat, gain_kvlat):
    qrank = gain_qlat.shape[0]
    kvrank = gain_kvlat.shape[0]
    scaled_rows = summed * lax.rsqrt(squares / full_width + epsilon)[:, None]
    query_latent = normed(scaled_rows[:, :qrank], gain_qlat).astype(jnp.bfloat16)
    new_latent = normed(scaled_rows[:, qrank : qrank + kvrank], gain_kvlat).astype(jnp.bfloat16)
    new_rope = scaled_rows[:, qrank + kvrank :].astype(jnp.bfloat16)
    return (query_latent, new_latent, new_rope)


def apply_values(numer_rows, value_map):
    return jnp.einsum("...hk,khv->...hv", numer_rows, value_map, precision=lax.Precision.HIGHEST)


def local(
    tokens,
    gain_in,
    w_qdown,
    w_kvdown,
    w_ropek,
    gain_qlat,
    gain_kvlat,
    w_qup,
    gain_q,
    w_ukey,
    w_uval,
    w_out,
    gain_out,
    cache_lat,
    cache_rope,
    parents,
    lengths,
    accepted,
):
    seq_count, proposals, local_width = tokens.shape
    full_width = local_width * lax.axis_size(("kv", "tp"))
    tok_rows = tokens.astype(jnp.float32).reshape(seq_count * proposals, local_width)
    scaled = (tok_rows * gain_in).astype(jnp.bfloat16)
    squares = jnp.sum(tok_rows * tok_rows, axis=-1)
    rope_rows = lax.dynamic_slice_in_dim(
        w_ropek, lax.axis_index(("kv", "tp")) * local_width, local_width, 0
    )
    joined = jnp.concatenate([w_qdown, w_kvdown, rope_rows], axis=1)
    partial_rows = jnp.dot(scaled, joined, preferred_element_type=jnp.float32)
    summed, total_squares = lax.psum((partial_rows, squares), ("kv", "tp"))
    query_latent, new_latent, new_rope = latents(
        summed, total_squares, full_width, gain_qlat, gain_kvlat
    )
    qrank = w_qup.shape[0]
    heads_here = w_qup.shape[1]
    qkhead = w_qup.shape[2]
    kvrank = w_ukey.shape[0]
    nope_dim = w_ukey.shape[2]
    vhead = w_uval.shape[2]
    rope_dim = cache_rope.shape[1]
    half_dim = rope_dim // 2
    reaches, depths = ancestry(parents)
    starts = lengths + accepted
    query_pos = starts[:, None] + depths
    queries = jnp.dot(
        query_latent, w_qup.reshape(qrank, heads_here * qkhead), preferred_element_type=jnp.float32
    )
    queries = normed(queries.reshape(seq_count, proposals, heads_here, qkhead), gain_q)
    query_nope = queries[..., :nope_dim].astype(jnp.bfloat16)
    angles = rope_angles(query_pos, half_dim)[:, :, None, :]
    cosine = jnp.cos(angles)
    sines = jnp.sin(angles)
    lower_half = queries[..., nope_dim : nope_dim + half_dim]
    upper_half = queries[..., nope_dim + half_dim :]
    query_rot = jnp.concatenate(
        [lower_half * cosine - upper_half * sines, upper_half * cosine + lower_half * sines],
        axis=-1,
    ).astype(jnp.bfloat16)
    query_lat = jnp.einsum(
        "sihn,khn->sihk", query_nope, w_ukey, preferred_element_type=jnp.float32
    ).astype(jnp.bfloat16)
    pos_count = cache_lat.shape[1]
    slots = lax.axis_index("kv") * pos_count + jnp.arange(pos_count, dtype=jnp.int32)
    offset = slots[None, :] - starts[:, None]
    inside = (offset >= 0) & (offset < proposals)
    matches = offset[:, :, None] == jnp.arange(proposals, dtype=jnp.int32)
    selector = matches.astype(jnp.bfloat16)
    new_latent = new_latent.reshape(seq_count, proposals, kvrank)
    new_rope = new_rope.reshape(seq_count, proposals, rope_dim)
    placed = jnp.einsum(
        "spj,sjk->spk", selector, new_latent, preferred_element_type=jnp.float32
    ).astype(jnp.bfloat16)
    lat_out = jnp.where(inside[:, :, None], placed, cache_lat)
    placed_rope = jnp.einsum(
        "spj,sjr->srp", selector, new_rope, preferred_element_type=jnp.float32
    ).astype(jnp.bfloat16)
    rope_out = jnp.where(inside[:, None, :], placed_rope, cache_rope)
    key_pos = jnp.where(
        inside,
        starts[:, None] + jnp.sum(jnp.where(matches, depths[:, None, :], 0), axis=-1),
        slots[None, :],
    )
    ancestor = jnp.einsum(
        "sij,spj->sip", reaches, matches.astype(jnp.float32), precision=lax.Precision.HIGHEST
    )
    visible = (offset < 0)[:, None, :] | (ancestor > 0.5)
    key_angles = jnp.swapaxes(rope_angles(key_pos, half_dim), 1, 2)
    key_cos = jnp.cos(key_angles)
    key_sin = jnp.sin(key_angles)
    rope32 = rope_out.astype(jnp.float32)
    key_low = rope32[:, :half_dim, :]
    key_high = rope32[:, half_dim:, :]
    key_rot = jnp.concatenate(
        [key_low * key_cos - key_high * key_sin, key_high * key_cos + key_low * key_sin], axis=1
    ).astype(jnp.bfloat16)
    scores = (
        jnp.einsum("sihk,spk->sihp", query_lat, lat_out, preferred_element_type=jnp.float32)
        + jnp.einsum("sihr,srp->sihp", query_rot, key_rot, preferred_element_type=jnp.float32)
    ) * qkhead ** (-0.5)
    masked = jnp.where(visible[:, :, None, :], scores, -jnp.inf)
    row_max = lax.pmax(jnp.max(masked, axis=-1), "kv")
    weights32 = jnp.exp(masked - row_max[..., None])
    denominator = jnp.sum(weights32, axis=-1)
    weights = weights32.astype(jnp.bfloat16)
    numerator = jnp.einsum("sihp,spk->sihk", weights, lat_out, preferred_element_type=jnp.float32)
    value_map = w_uval.astype(jnp.float32)
    numer_values = apply_values(numerator, value_map)
    values_all, denom_all = lax.psum((numer_values, denominator), "kv")
    head_out = (values_all / denom_all[..., None]).astype(jnp.bfloat16)
    head_rows = head_out.reshape(seq_count * proposals, heads_here * vhead)
    partial_out = jnp.dot(head_rows, w_out, preferred_element_type=jnp.float32).reshape(
        seq_count, proposals, w_out.shape[1]
    )
    mixed = lax.psum_scatter(partial_out, "tp", scatter_dimension=2, tiled=True)
    local_squares = jnp.sum(mixed * mixed, axis=-1)
    norm_total = lax.psum(local_squares, ("kv", "tp"))
    result = (mixed * lax.rsqrt(norm_total / full_width + epsilon)[..., None] * gain_out).astype(
        jnp.bfloat16
    )
    return (result, lat_out, rope_out)


def solution(mesh):
    placed = (
        P("dp", None, ("kv", "tp")),
        P(("kv", "tp")),
        P(("kv", "tp"), None),
        P(("kv", "tp"), None),
        P(),
        P(),
        P(),
        P(None, "tp", None),
        P(),
        P(None, "tp", None),
        P(None, "tp", None),
        P("tp", "kv"),
        P(("kv", "tp")),
        P("dp", "kv", None),
        P("dp", None, "kv"),
        P("dp", None),
        P("dp"),
        P("dp"),
    )
    return jax.shard_map(
        local,
        mesh=mesh,
        in_specs=placed,
        out_specs=(P("dp", None, ("kv", "tp")), P("dp", "kv", None), P("dp", None, "kv")),
        check_vma=False,
    )
```

profile of v0, /device:TPU:0, one launch (start us, length us, event | category | flops | bytes accessed | tf_op | source)
XLA Modules:
  0.0 292.3 jit_solution(4244914604734968146)
XLA Ops:
  7.3 0.8 constant_dynamic-slice_fusion
  8.2 0.9 fusion.43
  9.0 2.2 fusion.37
  11.7 5.6 %while.13 = (s32[]{:T(128)}, f32[16,16,16]{2,1,0:T(8,128)S(1)}, f32[16,16,16]{2,1,0:T(8,128)S(1)}, s32[16,16]{1,0:T(8,128)S(1)}, s32[]{:T(128)}) while((s32[]{:T(128)}, f32[16,16,16]{2,1,0:T(8,128)S(1)}, f32[16,16,16]{2,1,0:T(8,128)S(1)}, s32[16,16]{1,0:T(8,128)S(1)}, s32[]{:T(128)}) %tuple.45), condition=%wide.region_1.0_spmd.clone, body=%wide.region_0.0_spmd.clone.sunk | while | flops 798722 | bytes 99389 | solution.py:32
  17.6 35.1 %psum.36 = f32[256]{0:T(256)S(1)} all-reduce(f32[256]{0:T(256)S(1)} %reduce_sum.75), channel_id=1, replica_groups=mesh['dp'=2,'kv'=8,'tp'=2] {'kv','tp'}, use_global_device_ids=true, to_apply=%region_4.0 | all-reduce | flops 256 | bytes 2048 | tf_op jit(solution)/shard_map/psum | solution.py:81
  53.7 53.2 %all-reduce.3.cloned.1.call-done = f32[256,800]{0,1:T(8,128)} async-done(((f32[256,800]{0,1:T(8,128)}), f32[256,800]{0,1:T(8,128)}) %all-reduce.3.cloned.1.call-update) | async-done | bytes 819216 | tf_op jit(solution)/shard_map/psum | solution.py:81
  107.0 1.2 broadcast_multiply_fusion
  109.7 1.0 fusion.52
  110.7 1.1 fusion.31
  112.6 0.6 subtract_convert_fusion
  113.5 0.7 copy-done.2
  114.2 1.4 convert_select_fusion
  115.6 0.9 fusion.5
  116.5 2.0 fusion.53
  118.5 37.9 %pmax.7 = f32[16,16,8]{2,1,0:T(8,128)S(1)} all-reduce(f32[16,16,8]{2,1,0:T(8,128)S(1)} %get-tuple-element.61), channel_id=1, replica_groups=mesh['dp'=2,'kv'=8,'tp'=2] {'kv'}, use_global_device_ids=true, to_apply=%region_11.12 | all-reduce | flops 2048 | bytes 16384 | tf_op jit(solution)/shard_map/pmax | solution.py:152
  156.4 2.3 fusion.9
  159.7 2.1 convolution_bitcast_fusion
  161.9 35.7 %psum.38 = f32[16,16,8]{2,1,0:T(8,128)S(1)} all-reduce(f32[16,16,8]{2,1,0:T(8,128)S(1)} %get-tuple-element.47), channel_id=1, replica_groups=mesh['dp'=2,'kv'=8,'tp'=2] {'kv'}, use_global_device_ids=true, to_apply=%region_14.15 | all-reduce | flops 2048 | bytes 16384 | tf_op jit(solution)/shard_map/psum | solution.py:159
  197.8 41.0 %all-reduce.5.cloned.1.call-done = f32[16,16,8,128]{3,1,0,2:T(8,128)} async-done(((f32[16,16,8,128]{3,1,0,2:T(8,128)}), f32[16,16,8,128]{3,1,0,2:T(8,128)}) %all-reduce.5.cloned.1.call-update) | async-done | bytes 1048592 | tf_op jit(solution)/shard_map/psum | solution.py:159
  238.8 2.4 fusion.18
  241.2 7.5 %reduce-scatter.2.cloned.1.call-done = f32[16,16,128]{2,1,0:T(8,128)} async-done(((f32[16,16,256]{2,1,0:T(8,128)}), f32[16,16,128]{2,1,0:T(8,128)}) %reduce-scatter.2.cloned.1.call-update) | async-done | bytes 131088 | tf_op jit(solution)/shard_map/reduce_scatter | solution.py:165
  248.7 1.0 multiply_reduce_fusion.3
  249.7 34.4 %psum.39 = f32[16,16]{1,0:T(8,128)S(1)} all-reduce(f32[16,16]{1,0:T(8,128)S(1)} %multiply_reduce_fusion.3), channel_id=1, replica_groups=mesh['dp'=2,'kv'=8,'tp'=2] {'kv','tp'}, use_global_device_ids=true, to_apply=%region_17.18 | all-reduce | flops 256 | bytes 2048 | tf_op jit(solution)/shard_map/psum | solution.py:167
  284.1 1.6 multiply_convert_fusion.2
  (102 shorter events, 10.7 us)
Async XLA Ops:
  7.2 101.8 %copy-start = (bf16[512,8,96]{0,2,1:T(8,128)(2,1)S(1)}, bf16[512,8,96]{0,2,1:T(8,128)(2,1)}, u32[]{:S(2)}) copy-start(bf16[512,8,96]{0,2,1:T(8,128)(2,1)} %param.27) | copy-start | bytes 2359300
  7.2 4.1 %copy-start.6 = (bf16[16,16,128]{2,1,0:T(8,128)(2,1)S(1)}, bf16[16,16,128]{2,1,0:T(8,128)(2,1)}, u32[]{:S(2)}) copy-start(bf16[16,16,128]{2,1,0:T(8,128)(2,1)} %param.20) | copy-start | bytes 196612
  7.2 4.2 %copy-start.14 = (s32[16]{0:T(128)S(1)}, s32[16]{0:T(128)}, u32[]{:S(2)}) copy-start(s32[16]{0:T(128)} %param.37) | copy-start | bytes 196
  7.2 4.2 %copy-start.13 = (s32[16]{0:T(128)S(1)}, s32[16]{0:T(128)}, u32[]{:S(2)}) copy-start(s32[16]{0:T(128)} %param.36) | copy-start | bytes 196
  7.2 4.4 %copy-start.7 = (s32[16,16]{1,0:T(8,128)S(1)}, s32[16,16]{1,0:T(8,128)}, u32[]{:S(2)}) copy-start(s32[16,16]{1,0:T(8,128)} %param.35) | copy-start | bytes 3076
  7.2 99.7 %all-reduce.3.cloned.1.call-start = ((), (), s32[]{:S(2)}) async-start(), calls=%async_computation.1 | async-start | bytes 1638400 | tf_op jit(solution)/shard_map/psum | solution.py:81
  11.2 227.5 %all-reduce.5.cloned.1.call-start = ((), (), s32[]{:S(2)}) async-start(), calls=%async_computation.2 | async-start | bytes 2097152 | tf_op jit(solution)/shard_map/psum | solution.py:159
  17.3 91.2 %copy-start.8 = (f32[512]{0:T(512)S(1)}, f32[512]{0:T(512)}, u32[]{:S(2)}) copy-start(f32[512]{0:T(512)} %param.25) | copy-start | bytes 6148
  53.0 55.8 %copy-start.9 = (f32[256]{0:T(256)S(1)}, f32[256]{0:T(256)}, u32[]{:S(2)}) copy-start(f32[256]{0:T(256)} %param.26) | copy-start | bytes 3076
  108.5 1.2 copy-start.4
  109.0 2.8 copy-start.10
  109.6 2.5 copy-start.5
  112.6 1.6 copy-start.2
  115.6 43.1 %copy-start.1 = (bf16[16,256,256]{2,1,0:T(8,128)(2,1)}, bf16[16,256,256]{2,1,0:T(8,128)(2,1)S(1)}, u32[]{:S(2)}) copy-start(bf16[16,256,256]{2,1,0:T(8,128)(2,1)S(1)} %convert_select_fusion) | copy-start | bytes 6291460
  158.7 1.0 copy-start.3
  159.7 79.0 %copy-start.12 = (bf16[1024,256]{1,0:T(8,128)(2,1)S(1)}, bf16[1024,256]{1,0:T(8,128)(2,1)}, u32[]{:S(2)}) copy-start(bf16[1024,256]{1,0:T(8,128)(2,1)} %param.31) | copy-start | bytes 1572868
  161.9 86.8 %reduce-scatter.2.cloned.1.call-start = ((), (), s32[]{:S(2)}) async-start(), calls=%async_computation.3 | async-start | bytes 393216 | tf_op jit(solution)/shard_map/reduce_scatter | solution.py:165
  197.8 86.3 %copy-start.11 = (f32[128]{0:T(128)S(1)}, f32[128]{0:T(128)}, u32[]{:S(2)}) copy-start(f32[128]{0:T(128)} %param.32) | copy-start | bytes 1540
Sparse Core Ops, SparseCore 0:
  12.1 94.8 all-reduce.2
  162.0 76.7 all-reduce.4
  241.3 7.3 reduce-scatter.1
where the time goes:
time: 293 us; the launch traced here: 292 us
  blocking collectives  143 us (49%)
  waiting for transfers between devices  102 us (35%)
  matrix products  18.7 us (6%)
  between operations  14.2 us (5%)
  other arithmetic  11 us (4%)
    psum x1, waiting for transfers between devices, local(): summed, total_squares = lax.psum((partial_rows, squares), ('kv', 'tp'))  53.2 us
    psum x1, waiting for transfers between devices, local(): values_all, denom_all = lax.psum((numer_values, denominator), 'kv')  41 us
    pmax x1, blocking collectives, local(): row_max = lax.pmax(jnp.max(masked, axis=-1), 'kv')  37.9 us
    psum x1, blocking collectives, local(): values_all, denom_all = lax.psum((numer_values, denominator), 'kv')  35.7 us
    psum x1, blocking collectives, local(): summed, total_squares = lax.psum((partial_rows, squares), ('kv', 'tp'))  35.1 us
    psum x1, blocking collectives, local(): norm_total = lax.psum(local_squares, ('kv', 'tp'))  34.4 us
    reduce_scatter x1, waiting for transfers between devices, local(): mixed = lax.psum_scatter(partial_out, 'tp', scatter_dimension=2, tiled=True)  7.5 us
  transfers between devices with their start and end apart: 3, of which 3 were waited for; matrix products, arithmetic and copies ran while one was open for 2% of the time, Pallas kernels for 0%

commit v1 on v0

--- a/solution.py
+++ b/solution.py
@@ -4,6 +4,7 @@
 from jax.sharding import PartitionSpec as P
 
 epsilon = 1e-06
+supply_all_pages_over_axis = lambda x0: lax.all_gather(x0, ("kv", "tp")).sum(axis=0)
 
 
 def normed(values, gain_vec):
@@ -164,7 +165,7 @@
     )
     mixed = lax.psum_scatter(partial_out, "tp", scatter_dimension=2, tiled=True)
     local_squares = jnp.sum(mixed * mixed, axis=-1)
-    norm_total = lax.psum(local_squares, ("kv", "tp"))
+    norm_total = supply_all_pages_over_axis(local_squares)
     result = (mixed * lax.rsqrt(norm_total / full_width + epsilon)[..., None] * gain_out).astype(
         jnp.bfloat16
     )

time: 293 us -> 280 us (0.956)
  blocking collectives: 143 us -> 131 us
    psum x1 -> x0, blocking collectives: 34.4 us -> none  [local(): norm_total = lax.psum(local_squares, ('kv', 'tp'))]
    all_gather x0 -> x1, blocking collectives: none -> 21.9 us  [lax.all_gather(x0, ('kv', 'tp')).sum(axis=0)]
where the time goes in v1:
time: 280 us
  blocking collectives  131 us (47%)
  waiting for transfers between devices  102 us (36%)
  matrix products  18.7 us (7%)
  between operations  14.2 us (5%)
  other arithmetic  11 us (4%)
  local copies, waits for them, and re-layouts  2.92 us (1%)
    psum x1, waiting for transfers between devices, local(): summed, total_squares = lax.psum((partial_rows, squares), ('kv', 'tp'))  53.2 us
    psum x1, waiting for transfers between devices, local(): values_all, denom_all = lax.psum((numer_values, denominator), 'kv')  41 us
    pmax x1, blocking collectives, local(): row_max = lax.pmax(jnp.max(masked, axis=-1), 'kv')  37.9 us
    psum x1, blocking collectives, local(): values_all, denom_all = lax.psum((numer_values, denominator), 'kv')  35.7 us
    psum x1, blocking collectives, local(): summed, total_squares = lax.psum((partial_rows, squares), ('kv', 'tp'))  35.1 us
    all_gather x1, blocking collectives, lax.all_gather(x0, ('kv', 'tp')).sum(axis=0)  21.9 us
    reduce_scatter x1, waiting for transfers between devices, local(): mixed = lax.psum_scatter(partial_out, 'tp', scatter_dimension=2, tiled=True)  7.5 us
  transfers between devices with their start and end apart: 3, of which 3 were waited for; matrix products, arithmetic and copies ran while one was open for 2% of the time, Pallas kernels for 0%

profile of v1, /device:TPU:0, one launch (start us, length us, event | category | flops | bytes accessed | tf_op | source)
XLA Modules:
  0.0 279.8 jit_solution(1081908613193791656)
XLA Ops:
  7.3 0.8 constant_dynamic-slice_fusion
  8.2 0.9 fusion.43
  9.0 2.2 fusion.37
  11.7 5.6 %while.13 = (s32[]{:T(128)}, f32[16,16,16]{2,1,0:T(8,128)S(1)}, f32[16,16,16]{2,1,0:T(8,128)S(1)}, s32[16,16]{1,0:T(8,128)S(1)}, s32[]{:T(128)}) while((s32[]{:T(128)}, f32[16,16,16]{2,1,0:T(8,128)S(1)}, f32[16,16,16]{2,1,0:T(8,128)S(1)}, s32[16,16]{1,0:T(8,128)S(1)}, s32[]{:T(128)}) %tuple.45), condition=%wide.region_1.0_spmd.clone, body=%wide.region_0.0_spmd.clone.sunk | while | flops 798722 | bytes 99389 | solution.py:33
  17.6 35.1 %psum.29 = f32[256]{0:T(256)S(1)} all-reduce(f32[256]{0:T(256)S(1)} %reduce_sum.84), channel_id=1, replica_groups=mesh['dp'=2,'kv'=8,'tp'=2] {'kv','tp'}, use_global_device_ids=true, to_apply=%region_4.0 | all-reduce | flops 256 | bytes 2048 | tf_op jit(solution)/shard_map/psum | solution.py:82
  53.7 53.2 %all-reduce.3.cloned.1.call-done = f32[256,800]{0,1:T(8,128)} async-done(((f32[256,800]{0,1:T(8,128)}), f32[256,800]{0,1:T(8,128)}) %all-reduce.3.cloned.1.call-update) | async-done | bytes 819216 | tf_op jit(solution)/shard_map/psum | solution.py:82
  107.0 1.2 broadcast_multiply_fusion
  109.7 1.0 fusion.52
  110.7 1.1 fusion.31
  112.6 0.6 subtract_convert_fusion
  113.5 0.7 copy-done.2
  114.2 1.4 convert_select_fusion
  115.6 0.9 fusion.5
  116.5 2.0 fusion.53
  118.5 37.9 %pmax.7 = f32[16,16,8]{2,1,0:T(8,128)S(1)} all-reduce(f32[16,16,8]{2,1,0:T(8,128)S(1)} %get-tuple-element.61), channel_id=1, replica_groups=mesh['dp'=2,'kv'=8,'tp'=2] {'kv'}, use_global_device_ids=true, to_apply=%region_11.12 | all-reduce | flops 2048 | bytes 16384 | tf_op jit(solution)/shard_map/pmax | solution.py:153
  156.4 2.3 fusion.9
  159.7 2.1 convolution_bitcast_fusion
  161.9 35.7 %psum.31 = f32[16,16,8]{2,1,0:T(8,128)S(1)} all-reduce(f32[16,16,8]{2,1,0:T(8,128)S(1)} %get-tuple-element.47), channel_id=1, replica_groups=mesh['dp'=2,'kv'=8,'tp'=2] {'kv'}, use_global_device_ids=true, to_apply=%region_14.15 | all-reduce | flops 2048 | bytes 16384 | tf_op jit(solution)/shard_map/psum | solution.py:160
  197.8 41.0 %all-reduce.5.cloned.1.call-done = f32[16,16,8,128]{3,1,0,2:T(8,128)} async-done(((f32[16,16,8,128]{3,1,0,2:T(8,128)}), f32[16,16,8,128]{3,1,0,2:T(8,128)}) %all-reduce.5.cloned.1.call-update) | async-done | bytes 1048592 | tf_op jit(solution)/shard_map/psum | solution.py:160
  238.8 2.4 fusion.18
  241.2 7.5 %reduce-scatter.2.cloned.1.call-done = f32[16,16,128]{2,1,0:T(8,128)} async-done(((f32[16,16,256]{2,1,0:T(8,128)}), f32[16,16,128]{2,1,0:T(8,128)}) %reduce-scatter.2.cloned.1.call-update) | async-done | bytes 131088 | tf_op jit(solution)/shard_map/reduce_scatter | solution.py:166
  248.7 1.0 multiply_reduce_fusion.3
  249.7 21.9 %all-gather = f32[256,16]{1,0:T(8,128)S(1)} all-gather(f32[16,16]{1,0:T(8,128)S(1)} %multiply_reduce_fusion.3), channel_id=2, replica_groups=mesh['dp'=2,'kv'=8,'tp'=2] {'kv','tp'}, dimensions={0}, use_global_device_ids=true | all-gather | bytes 17408 | tf_op jit(solution)/shard_map/all_gather | solution.py:7
  271.6 1.6 multiply_convert_fusion.2
  (103 shorter events, 10.7 us)
Async XLA Ops:
  7.2 101.8 %copy-start = (bf16[512,8,96]{0,2,1:T(8,128)(2,1)S(1)}, bf16[512,8,96]{0,2,1:T(8,128)(2,1)}, u32[]{:S(2)}) copy-start(bf16[512,8,96]{0,2,1:T(8,128)(2,1)} %param.27) | copy-start | bytes 2359300
  7.2 4.1 %copy-start.6 = (bf16[16,16,128]{2,1,0:T(8,128)(2,1)S(1)}, bf16[16,16,128]{2,1,0:T(8,128)(2,1)}, u32[]{:S(2)}) copy-start(bf16[16,16,128]{2,1,0:T(8,128)(2,1)} %param.20) | copy-start | bytes 196612
  7.2 4.2 %copy-start.14 = (s32[16]{0:T(128)S(1)}, s32[16]{0:T(128)}, u32[]{:S(2)}) copy-start(s32[16]{0:T(128)} %param.37) | copy-start | bytes 196
  7.2 4.2 %copy-start.13 = (s32[16]{0:T(128)S(1)}, s32[16]{0:T(128)}, u32[]{:S(2)}) copy-start(s32[16]{0:T(128)} %param.36) | copy-start | bytes 196
  7.2 4.4 %copy-start.7 = (s32[16,16]{1,0:T(8,128)S(1)}, s32[16,16]{1,0:T(8,128)}, u32[]{:S(2)}) copy-start(s32[16,16]{1,0:T(8,128)} %param.35) | copy-start | bytes 3076
  7.2 99.7 %all-reduce.3.cloned.1.call-start = ((), (), s32[]{:S(2)}) async-start(), calls=%async_computation.1 | async-start | bytes 1638400 | tf_op jit(solution)/shard_map/psum | solution.py:82
  11.2 227.5 %all-reduce.5.cloned.1.call-start = ((), (), s32[]{:S(2)}) async-start(), calls=%async_computation.2 | async-start | bytes 2097152 | tf_op jit(solution)/shard_map/psum | solution.py:160
  17.3 91.2 %copy-start.8 = (f32[512]{0:T(512)S(1)}, f32[512]{0:T(512)}, u32[]{:S(2)}) copy-start(f32[512]{0:T(512)} %param.25) | copy-start | bytes 6148
  53.0 55.8 %copy-start.9 = (f32[256]{0:T(256)S(1)}, f32[256]{0:T(256)}, u32[]{:S(2)}) copy-start(f32[256]{0:T(256)} %param.26) | copy-start | bytes 3076
  108.5 1.2 copy-start.4
  109.0 2.8 %copy-start.10 = (f32[96]{0:T(128)S(1)}, f32[96]{0:T(128)}, u32[]{:S(2)}) copy-start(f32[96]{0:T(128)} %param.28) | copy-start | bytes 1156
  109.6 2.5 copy-start.5
  112.6 1.6 copy-start.2
  115.6 43.1 %copy-start.1 = (bf16[16,256,256]{2,1,0:T(8,128)(2,1)}, bf16[16,256,256]{2,1,0:T(8,128)(2,1)S(1)}, u32[]{:S(2)}) copy-start(bf16[16,256,256]{2,1,0:T(8,128)(2,1)S(1)} %convert_select_fusion) | copy-start | bytes 6291460
  158.7 1.0 copy-start.3
  159.7 79.0 %copy-start.12 = (bf16[1024,256]{1,0:T(8,128)(2,1)S(1)}, bf16[1024,256]{1,0:T(8,128)(2,1)}, u32[]{:S(2)}) copy-start(bf16[1024,256]{1,0:T(8,128)(2,1)} %param.31) | copy-start | bytes 1572868
  161.9 86.8 %reduce-scatter.2.cloned.1.call-start = ((), (), s32[]{:S(2)}) async-start(), calls=%async_computation.3 | async-start | bytes 393216 | tf_op jit(solution)/shard_map/reduce_scatter | solution.py:166
  197.8 73.9 %copy-start.11 = (f32[128]{0:T(128)S(1)}, f32[128]{0:T(128)}, u32[]{:S(2)}) copy-start(f32[128]{0:T(128)} %param.32) | copy-start | bytes 1540
Sparse Core Ops, SparseCore 0:
  12.1 94.8 all-reduce.2
  162.0 76.7 all-reduce.4
  241.3 7.3 reduce-scatter.1
